TPU v7x, 32 devices: a whole 2x2x4 slice. The times are simulated.
32 devices in a mesh: rep: 4 (over z), fs: 4 (over y, x), tp: 2 (over core).
Axes of the slice: x: 2, y: 2, z: 4, core: 2. Of those that a mesh axis runs over, the one named last changes fastest.
Arguments:
- tokens: bfloat16 [2048, 1024], P(('rep', 'fs', 'tp')), may hold values from -6 to 6
- cotangent: bfloat16 [2048, 1024], P(('rep', 'fs', 'tp')), may hold values from -6 to 6
- gate_weight: bfloat16 [1024, 2816], P('fs', 'tp'), may hold values from -0.1875 to 0.1875
- up_weight: bfloat16 [1024, 2816], P('fs', 'tp'), may hold values from -0.1875 to 0.1875
- down_weight: bfloat16 [2816, 1024], P('tp', 'fs'), may hold values from -0.109375 to 0.109375
Outputs:
- input_grad: bfloat16 [2048, 1024], P(('rep', 'fs', 'tp'))
- gate_grad: float32 [1024, 2816], P('fs', 'tp')
- up_grad: float32 [1024, 2816], P('fs', 'tp')
- down_grad: float32 [2816, 1024], P('tp', 'fs')
- gate_power: float32 [1024], P('fs')
- up_power: float32 [1024], P('fs')
- down_power: float32 [2816], P('tp')
All inputs are finite; a program needn't handle non-finite values.
Results may differ from a plain program's by a relative error of at most 0.0017.
Values may be sent and summed in bfloat16 or wider, within the bound.
A program may use at most 64 MiB of HBM per device.

v0:
```python
import math
import jax
import jax.numpy as jnp
from jax import lax
from jax.sharding import PartitionSpec as P

D = 1024
FF = 2816
EPSILON = 1e-06


def contract_rows(left, right):
    return lax.dot_general(
        left, right, (((0,), (0,)), ((), ())), preferred_element_type=jnp.float32
    )


def contract_cols(left, right):
    return lax.dot_general(
        left, right, (((1,), (1,)), ((), ())), preferred_element_type=jnp.float32
    )


def on_device(tokens, cotangent, gate_weight, up_weight, down_weight):
    tp_count = lax.axis_size("tp")
    fs_count = lax.axis_size("fs")
    rep_count = lax.axis_size("rep")
    width = tokens.shape[1]
    factor = 1.0 / math.sqrt(tokens.shape[0] * tp_count * fs_count * rep_count)
    xfloat = tokens.astype(jnp.float32)
    recip_norm = lax.rsqrt(jnp.mean(xfloat * xfloat, axis=1, keepdims=True) + EPSILON)
    normed_exact = xfloat * recip_norm
    normed = normed_exact.astype(jnp.bfloat16)
    group_normed, group_cotangent = (
        lax.all_gather(normed, "tp", axis=0, tiled=True),
        lax.all_gather(cotangent, "tp", axis=0, tiled=True),
    )
    gate_full, up_full, down_full = (
        lax.all_gather(gate_weight, "fs", axis=0, tiled=True),
        lax.all_gather(up_weight, "fs", axis=0, tiled=True),
        lax.all_gather(down_weight.T, "fs", axis=0, tiled=True),
    )
    gate_pre = jnp.dot(group_normed, gate_full, preferred_element_type=jnp.float32)
    up_pre = jnp.dot(group_normed, up_full, preferred_element_type=jnp.float32)
    sigmoid_gate = jax.nn.sigmoid(gate_pre)
    activated = gate_pre * sigmoid_gate
    hidden = (activated * up_pre).astype(jnp.bfloat16)
    grad_hidden = 0.5 * jnp.dot(group_cotangent, down_full, preferred_element_type=jnp.float32)
    grad_up_pre = (grad_hidden * activated).astype(jnp.bfloat16)
    grad_gate_pre = (
        grad_hidden * up_pre * sigmoid_gate * (1.0 + gate_pre * (1.0 - sigmoid_gate))
    ).astype(jnp.bfloat16)
    normed_part = contract_cols(grad_gate_pre, gate_full) + contract_cols(grad_up_pre, up_full)
    grad_normed = lax.psum_scatter(normed_part, "tp", scatter_dimension=0, tiled=True)
    inner = jnp.mean(grad_normed * normed_exact, axis=1, keepdims=True)
    input_grad = (recip_norm * (grad_normed - normed_exact * inner)).astype(jnp.bfloat16)
    hidden_local = gate_weight.shape[1]

    def rows_term():
        normed_cols = lax.slice_in_dim(
            group_normed, 0, width // fs_count * lax.axis_size("fs"), axis=1
        )
        cotangent_cols = lax.slice_in_dim(
            group_cotangent, 0, width // fs_count * lax.axis_size("fs"), axis=1
        )
        return factor * jnp.concatenate(
            [
                contract_rows(normed_cols, grad_gate_pre),
                contract_rows(normed_cols, grad_up_pre),
                0.5 * contract_rows(cotangent_cols, hidden),
            ],
            axis=1,
        )

    reduced = lax.psum_scatter(rows_term(), "fs", scatter_dimension=0, tiled=True)
    reduced = lax.psum(reduced, "rep")
    gate_grad = reduced[:, :hidden_local]
    up_grad = reduced[:, hidden_local : 2 * hidden_local]
    down_grad = reduced[:, 2 * hidden_local :].T
    gate_sums, up_sums = lax.psum(
        (jnp.sum(gate_grad * gate_grad, axis=1), jnp.sum(up_grad * up_grad, axis=1)), "tp"
    )
    down_sums = lax.psum(jnp.sum(down_grad * down_grad, axis=1), "fs")
    return (input_grad, gate_grad, up_grad, down_grad, gate_sums / FF, up_sums / FF, down_sums / D)


def solution(mesh):
    placed = (
        P(("rep", "fs", "tp"), None),
        P(("rep", "fs", "tp"), None),
        P("fs", "tp"),
        P("fs", "tp"),
        P("tp", "fs"),
    )
    return jax.shard_map(
        on_device,
        mesh=mesh,
        in_specs=placed,
        out_specs=(
            P(("rep", "fs", "tp"), None),
            P("fs", "tp"),
            P("fs", "tp"),
            P("tp", "fs"),
            P("fs"),
            P("fs"),
            P("tp"),
        ),
        check_vma=False,
    )
```

profile of v0, /device:TPU:0, one launch (start us, length us, event | category | flops | bytes accessed | tf_op | source)
XLA Modules:
  0.0 513.0 jit_solution(5771994517067918810)
XLA Ops:
  7.2 0.0 all-gather.8.cloned.1.call-start
  7.2 0.7 all-gather.8.cloned.1.call-update
  7.9 0.0 all-gather.6.cloned.1.call-start
  8.0 0.7 all-gather.6.cloned.1.call-update
  8.7 0.0 all-gather.4.cloned.1.call-start
  8.7 0.7 all-gather.4.cloned.1.call-update
  9.4 0.0 reduce-scatter.5.cloned.1.call-start
  9.4 1.0 fusion.8
  10.5 1.0 fusion.3
  11.5 2.1 all_gather.17
  13.6 2.0 all_gather.15
  15.6 38.7 %all-gather.8.cloned.1.call-done = bf16[1024,1408]{1,0:T(8,128)(2,1)} async-done(((bf16[256,1408]{1,0:T(8,128)(2,1)}), bf16[1024,1408]{1,0:T(8,128)(2,1)}) %all-gather.8.cloned.1.call-update) | async-done | bytes 2883600 | tf_op jit(solution)/shard_map/all_gather | solution.py:39
  54.3 2.4 fusion.12
  56.7 41.1 %all-gather.6.cloned.1.call-done = bf16[1024,1408]{1,0:T(8,128)(2,1)} async-done(((bf16[256,1408]{1,0:T(8,128)(2,1)}), bf16[1024,1408]{1,0:T(8,128)(2,1)}) %all-gather.6.cloned.1.call-update) | async-done | bytes 2883600 | tf_op jit(solution)/shard_map/all_gather | solution.py:40
  97.8 2.4 fusion.11
  100.2 3.5 multiply_bitcast_fusion
  103.7 37.5 %all-gather.4.cloned.1.call-done = bf16[1024,1408]{0,1:T(8,128)(2,1)} async-done(((bf16[256,1408]{0,1:T(8,128)(2,1)}), bf16[1024,1408]{0,1:T(8,128)(2,1)}) %all-gather.4.cloned.1.call-update) | async-done | bytes 2883600 | tf_op jit(solution)/shard_map/all_gather | solution.py:41
  141.2 2.9 multiply_convert_fusion.1
  144.1 0.0 copy-start.3
  144.2 0.9 fusion.15
  145.1 0.0 slice-start
  145.1 0.0 slice-start.1
  145.1 0.9 fusion.14
  146.1 1.2 slice-done
  147.3 0.5 slice-done.1
  147.8 6.3 %maximum_multiply_fusion = f32[1024,4224]{1,0:T(8,128)} fusion(f32[1024,1408]{1,0:T(8,128)S(1)} %bitcast.23, f32[1024,1408]{1,0:T(8,128)S(1)} %fusion.15, f32[1024,1408]{1,0:T(8,128)S(1)} %fusion.14), kind=kLoop, calls=%fused_computation | loop fusion | flops 12976128 | bytes 34603008 | tf_op jit(solution)/shard_map/mul | solution.py:66
  154.1 0.0 reduce-scatter.5.cloned.1.call-update
  154.1 0.0 reduce-scatter.3.cloned.1.call-start
  154.2 1.7 copy-done
  155.9 1.0 fusion.13
  157.0 0.8 copy-done.1
  157.7 0.0 copy-done.4
  157.7 1.8 convolution_add_fusion
  159.6 0.0 reduce-scatter.3.cloned.1.call-update
  159.6 0.0 all-reduce.3.cloned.1.call-start
  159.7 152.6 %reduce-scatter.5.cloned.1.call-done = f32[256,4224]{1,0:T(8,128)} async-done(((f32[1024,4224]{1,0:T(8,128)}), f32[256,4224]{1,0:T(8,128)}) %reduce-scatter.5.cloned.1.call-update) | async-done | bytes 4325392 | tf_op jit(solution)/shard_map/reduce_scatter | solution.py:75
  312.3 0.0 all-reduce.3.cloned.1.call-update
  312.3 10.6 %reduce-scatter.3.cloned.1.call-done = f32[64,1024]{1,0:T(8,128)} async-done(((f32[128,1024]{1,0:T(8,128)}), f32[64,1024]{1,0:T(8,128)}) %reduce-scatter.3.cloned.1.call-update) | async-done | bytes 262160 | tf_op jit(solution)/shard_map/reduce_scatter | solution.py:54
  322.9 1.2 fusion.4
  324.0 1.7 fusion.7
  325.8 159.7 %all-reduce.3.cloned.1.call-done = f32[256,4224]{1,0:T(8,128)} async-done(((f32[256,4224]{1,0:T(8,128)}), f32[256,4224]{1,0:T(8,128)}) %all-reduce.3.cloned.1.call-update) | async-done | bytes 4325392 | tf_op jit(solution)/shard_map/psum | solution.py:76
  485.5 1.5 multiply_reduce_fusion
  487.0 10.1 %psum.31 = f32[1408]{0:T(1024)S(1)} all-reduce(f32[1408]{0:T(1024)S(1)} %multiply_reduce_fusion), channel_id=1, replica_groups=mesh['rep'=4,'fs'=4,'tp'=2] {'fs'}, use_global_device_ids=true, to_apply=%region_10.0 | all-reduce | flops 1408 | bytes 11264 | tf_op jit(solution)/shard_map/psum | solution.py:83
  497.0 0.6 broadcast_multiply_fusion
  497.6 3.9 multiply_reduce_fusion.1
  501.6 1.5 copy.13
  503.1 2.4 all-reduce
  505.5 0.6 broadcast_multiply_fusion.1
  (11 shorter events, 0.0 us)
Async XLA Ops:
  7.2 6.5 %copy-start.5 = (bf16[64,1024]{1,0:T(8,128)(2,1)S(1)}, bf16[64,1024]{1,0:T(8,128)(2,1)}, u32[]{:S(2)}) copy-start(bf16[64,1024]{1,0:T(8,128)(2,1)} %param.6) | copy-start | bytes 393220
  7.2 47.1 %all-gather.8.cloned.1.call-start = ((), (), s32[]{:S(2)}) async-start(), calls=%async_computation.4 | async-start | bytes 3604480 | tf_op jit(solution)/shard_map/all_gather | solution.py:39
  7.9 89.9 %all-gather.6.cloned.1.call-start = ((), (), s32[]{:S(2)}) async-start(), calls=%async_computation.3 | async-start | bytes 3604480 | tf_op jit(solution)/shard_map/all_gather | solution.py:40
  8.7 132.5 %all-gather.4.cloned.1.call-start = ((), (), s32[]{:S(2)}) async-start(), calls=%async_computation.2 | async-start | bytes 3604480 | tf_op jit(solution)/shard_map/all_gather | solution.py:41
  9.4 302.9 %reduce-scatter.5.cloned.1.call-start = ((), (), s32[]{:S(2)}) async-start(), calls=%async_computation.6 | async-start | bytes 21626880 | tf_op jit(solution)/shard_map/reduce_scatter | solution.py:75
  144.1 1.0 copy-start.3
  145.1 2.2 slice-start
  145.1 2.7 slice-start.1
  154.1 1.8 copy-start
  154.1 168.8 %reduce-scatter.3.cloned.1.call-start = ((), (), s32[]{:S(2)}) async-start(), calls=%async_computation.5 | async-start | bytes 786432 | tf_op jit(solution)/shard_map/reduce_scatter | solution.py:54
  155.9 1.8 copy-start.1
  155.9 1.8 copy-start.4
  159.6 163.3 %copy-start.2 = (bf16[64,1024]{1,0:T(8,128)(2,1)S(1)}, bf16[64,1024]{1,0:T(8,128)(2,1)}, u32[]{:S(2)}) copy-start(bf16[64,1024]{1,0:T(8,128)(2,1)} %param.5) | copy-start | bytes 393220
  159.6 325.9 %all-reduce.3.cloned.1.call-start = ((), (), s32[]{:S(2)}) async-start(), calls=%async_computation.7 | async-start | bytes 8650752 | tf_op jit(solution)/shard_map/psum | solution.py:76
Sparse Core Ops, SparseCore 0:
  9.8 44.3 all-gather.7
  56.1 41.6 all-gather.5
  99.6 41.5 all-gather.3
  154.2 157.9 reduce-scatter.4
  314.9 7.9 reduce-scatter.2
  325.1 160.3 all-reduce.2
where the time goes:
time: 513 us
  waiting for transfers between devices  442 us (86%)
  other arithmetic  17.8 us (3%)
  blocking collectives  16.6 us (3%)
  matrix products  16 us (3%)
  between operations  14.2 us (3%)
  local copies, waits for them, and re-layouts  5.81 us (1%)
    psum x1, waiting for transfers between devices, on_device(): reduced = lax.psum(reduced, 'rep')  160 us
    reduce_scatter x1, waiting for transfers between devices, on_device(): lax.psum_scatter(rows_term(), 'fs', scatter_dimension=0, tiled=True)  153 us
    all_gather x1, waiting for transfers between devices, on_device(): lax.all_gather(up_weight, 'fs', axis=0, tiled=True)  41.1 us
    all_gather x1, waiting for transfers between devices, on_device(): lax.all_gather(gate_weight, 'fs', axis=0, tiled=True)  38.7 us
    all_gather x1, waiting for transfers between devices, on_device(): lax.all_gather(down_weight.T, 'fs', axis=0, tiled=True)  37.5 us
    reduce_scatter x1, waiting for transfers between devices, on_device(): lax.psum_scatter(normed_part, 'tp', scatter_dimension=0, tiled=True)  10.6 us
  transfers between devices with their start and end apart: 6, of which 6 were waited for; matrix products, arithmetic and copies ran while one was open for 3% of the time, Pallas kernels for 0%

commit v1 on v0

--- a/solution.py
+++ b/solution.py
@@ -73,7 +73,7 @@
         )
 
     reduced = lax.psum_scatter(rows_term(), "fs", scatter_dimension=0, tiled=True)
-    reduced = lax.psum(reduced, "rep")
+    reduced = jnp.sum(lax.all_gather(reduced, "rep"), axis=0)
     gate_grad = reduced[:, :hidden_local]
     up_grad = reduced[:, hidden_local : 2 * hidden_local]
     down_grad = reduced[:, 2 * hidden_local :].T

time: 513 us -> 660 us (1.29)
  waiting for transfers between devices: 442 us -> 579 us
  other arithmetic: 17.8 us -> 27.1 us
    all_gather x0 -> x1, waiting for transfers between devices: none -> 297 us  [on_device(): reduced = jnp.sum(lax.all_gather(reduced, 'rep'), axis=0)]
    psum x1 -> x0, waiting for transfers between devices: 160 us -> none  [on_device(): reduced = lax.psum(reduced, 'rep')]
    reduce_sum x0 -> x1, other arithmetic: none -> 9.34 us  [on_device(): reduced = jnp.sum(lax.all_gather(reduced, 'rep'), axis=0)]
  transfers between devices with their start and end apart: 6 -> 6, of which waited for: 6 -> 6; matrix products, arithmetic and copies ran while one was open for 3% -> 2% of each run, Pallas kernels for 0% -> 0%
where the time goes in v1:
time: 660 us; the launch traced here: 659 us
  waiting for transfers between devices  579 us (88%)
  other arithmetic  27.1 us (4%)
  blocking collectives  16.6 us (3%)
  matrix products  15.9 us (2%)
  between operations  14.2 us (2%)
    all_gather x1, waiting for transfers between devices, on_device(): reduced = jnp.sum(lax.all_gather(reduced, 'rep'), axis=0)  297 us
    reduce_scatter x1, waiting for transfers between devices, on_device(): lax.psum_scatter(rows_term(), 'fs', scatter_dimension=0, tiled=True)  153 us
    all_gather x1, waiting for transfers between devices, on_device(): lax.all_gather(up_weight, 'fs', axis=0, tiled=True)  41.1 us
    all_gather x1, waiting for transfers between devices, on_device(): lax.all_gather(gate_weight, 'fs', axis=0, tiled=True)  38.7 us
    all_gather x1, waiting for transfers between devices, on_device(): lax.all_gather(down_weight.T, 'fs', axis=0, tiled=True)  37.5 us
  transfers between devices with their start and end apart: 6, of which 6 were waited for; matrix products, arithmetic and copies ran while one was open for 2% of the time, Pallas kernels for 0%

profile of v1, /device:TPU:0, one launch (start us, length us, event | category | flops | bytes accessed | tf_op | source)
XLA Modules:
  0.0 659.1 jit_solution(585346418188631449)
XLA Ops:
  7.2 0.0 all-gather.10.cloned.1.call-start
  7.2 0.7 all-gather.10.cloned.1.call-update
  7.9 0.0 all-gather.8.cloned.1.call-start
  8.0 0.7 all-gather.8.cloned.1.call-update
  8.7 0.0 all-gather.6.cloned.1.call-start
  8.7 0.7 all-gather.6.cloned.1.call-update
  9.4 0.0 reduce-scatter.5.cloned.1.call-start
  9.4 1.0 fusion.8
  10.5 1.0 fusion.3
  11.5 2.1 all_gather.23
  13.6 2.0 all_gather.21
  15.6 38.7 %all-gather.10.cloned.1.call-done = bf16[1024,1408]{1,0:T(8,128)(2,1)} async-done(((bf16[256,1408]{1,0:T(8,128)(2,1)}), bf16[1024,1408]{1,0:T(8,128)(2,1)}) %all-gather.10.cloned.1.call-update) | async-done | bytes 2883600 | tf_op jit(solution)/shard_map/all_gather | solution.py:39
  54.3 2.4 fusion.12
  56.7 41.1 %all-gather.8.cloned.1.call-done = bf16[1024,1408]{1,0:T(8,128)(2,1)} async-done(((bf16[256,1408]{1,0:T(8,128)(2,1)}), bf16[1024,1408]{1,0:T(8,128)(2,1)}) %all-gather.8.cloned.1.call-update) | async-done | bytes 2883600 | tf_op jit(solution)/shard_map/all_gather | solution.py:40
  97.8 2.4 fusion.11
  100.2 3.5 multiply_bitcast_fusion
  103.7 37.5 %all-gather.6.cloned.1.call-done = bf16[1024,1408]{0,1:T(8,128)(2,1)} async-done(((bf16[256,1408]{0,1:T(8,128)(2,1)}), bf16[1024,1408]{0,1:T(8,128)(2,1)}) %all-gather.6.cloned.1.call-update) | async-done | bytes 2883600 | tf_op jit(solution)/shard_map/all_gather | solution.py:41
  141.2 2.9 multiply_convert_fusion.1
  144.1 0.0 copy-start.3
  144.2 0.9 fusion.15
  145.1 0.0 slice-start.1
  145.1 0.9 fusion.14
  146.1 1.2 slice-done
  147.3 0.5 slice-done.1
  147.8 6.3 maximum_multiply_fusion
  154.1 0.0 reduce-scatter.5.cloned.1.call-update
  154.1 0.0 reduce-scatter.3.cloned.1.call-start
  154.1 1.7 copy-done
  155.9 1.0 fusion.13
  156.9 0.8 copy-done.1
  157.7 0.0 copy-done.4
  157.7 1.9 convolution_add_fusion
  159.6 0.0 reduce-scatter.3.cloned.1.call-update
  159.6 0.0 all-gather.12.cloned.1.call-start
  159.7 152.6 %reduce-scatter.5.cloned.1.call-done = f32[256,4224]{1,0:T(8,128)} async-done(((f32[1024,4224]{1,0:T(8,128)}), f32[256,4224]{1,0:T(8,128)}) %reduce-scatter.5.cloned.1.call-update) | async-done | bytes 4325392 | tf_op jit(solution)/shard_map/reduce_scatter | solution.py:75
  312.2 0.0 all-gather.12.cloned.1.call-update
  312.3 10.6 %reduce-scatter.3.cloned.1.call-done = f32[64,1024]{1,0:T(8,128)} async-done(((f32[128,1024]{1,0:T(8,128)}), f32[64,1024]{1,0:T(8,128)}) %reduce-scatter.3.cloned.1.call-update) | async-done | bytes 262160 | tf_op jit(solution)/shard_map/reduce_scatter | solution.py:54
  322.9 1.2 fusion.4
  324.0 1.7 fusion.7
  325.8 296.6 %all-gather.12.cloned.1.call-done = f32[1024,4224]{1,0:T(8,128)} async-done(((f32[256,4224]{1,0:T(8,128)}), f32[1024,4224]{1,0:T(8,128)}) %all-gather.12.cloned.1.call-update) | async-done | bytes 17301520 | tf_op jit(solution)/shard_map/all_gather | solution.py:76
  622.3 9.3 %reduce_sum.56 = f32[256,4224]{1,0:T(8,128)} reduce(f32[4,256,4224]{2,1,0:T(8,128)} %bitcast.25, f32[]{:T(128)} %constant.7.clone.1), dimensions={0}, to_apply=%region_4.0 | reduce | flops 3244032 | bytes 21626884 | tf_op jit(solution)/shard_map/reduce_sum | solution.py:76
  631.7 1.5 multiply_reduce_fusion
  633.2 3.9 multiply_reduce_fusion.1
  637.1 10.0 %psum.23 = f32[1408]{0:T(1024)S(1)} all-reduce(f32[1408]{0:T(1024)S(1)} %multiply_reduce_fusion), channel_id=1, replica_groups=mesh['rep'=4,'fs'=4,'tp'=2] {'fs'}, use_global_device_ids=true, to_apply=%region_10.0 | all-reduce | flops 1408 | bytes 11264 | tf_op jit(solution)/shard_map/psum | solution.py:83
  647.1 0.6 broadcast_multiply_fusion
  647.7 1.5 copy.16
  649.3 2.4 all-reduce
  651.7 0.6 broadcast_multiply_fusion.1
  (12 shorter events, 0.0 us)
Async XLA Ops:
  7.2 6.5 copy-start.5
  7.2 47.1 %all-gather.10.cloned.1.call-start = ((), (), s32[]{:S(2)}) async-start(), calls=%async_computation.4 | async-start | bytes 3604480 | tf_op jit(solution)/shard_map/all_gather | solution.py:39
  7.9 89.9 %all-gather.8.cloned.1.call-start = ((), (), s32[]{:S(2)}) async-start(), calls=%async_computation.3 | async-start | bytes 3604480 | tf_op jit(solution)/shard_map/all_gather | solution.py:40
  8.7 132.5 %all-gather.6.cloned.1.call-start = ((), (), s32[]{:S(2)}) async-start(), calls=%async_computation.2 | async-start | bytes 3604480 | tf_op jit(solution)/shard_map/all_gather | solution.py:41
  9.4 302.8 %reduce-scatter.5.cloned.1.call-start = ((), (), s32[]{:S(2)}) async-start(), calls=%async_computation.6 | async-start | bytes 21626880 | tf_op jit(solution)/shard_map/reduce_scatter | solution.py:75
  144.1 1.0 copy-start.3
  145.1 2.2 slice-start
  145.1 2.7 slice-start.1
  154.1 1.8 copy-start
  154.1 168.8 %reduce-scatter.3.cloned.1.call-start = ((), (), s32[]{:S(2)}) async-start(), calls=%async_computation.5 | async-start | bytes 786432 | tf_op jit(solution)/shard_map/reduce_scatter | solution.py:54
  155.9 1.8 copy-start.1
  155.9 1.8 copy-start.4
  159.6 163.3 %copy-start.2 = (bf16[64,1024]{1,0:T(8,128)(2,1)S(1)}, bf16[64,1024]{1,0:T(8,128)(2,1)}, u32[]{:S(2)}) copy-start(bf16[64,1024]{1,0:T(8,128)(2,1)} %param.5) | copy-start | bytes 393220
  159.6 462.7 %all-gather.12.cloned.1.call-start = ((), (), s32[]{:S(2)}) async-start(), calls=%async_computation.7 | async-start | bytes 21626880 | tf_op jit(solution)/shard_map/all_gather | solution.py:76
Sparse Core Ops, SparseCore 0:
  9.8 44.3 all-gather.9
  56.1 41.6 all-gather.7
  99.6 41.5 all-gather.5
  154.2 157.9 reduce-scatter.4
  314.9 7.9 reduce-scatter.2
  324.3 297.9 all-gather.11
